TPU v7x, 32 devices: a whole 2x2x4 slice. The times are simulated.
32 devices in a mesh: ep: 8 (over z, x), tp: 4 (over y, core).
Axes of the slice: x: 2, y: 2, z: 4, core: 2. Of those that a mesh axis runs over, the one named last changes fastest.
Arguments:
- mixer_in: bfloat16 [1024, 2048], P('ep'), may hold values from -6 to 6
- mixer_gain: float32 [2048], replicated, may hold values from 0.1 to 1.9
- w_value: bfloat16 [2048, 1536], P(None, 'tp'), may hold values from -0.125 to 0.125
- w_gate: bfloat16 [2048, 1536], P(None, 'tp'), may hold values from -0.125 to 0.125
- w_taps: float32 [31, 1536], P(None, 'tp'), may hold values from -3 to 3
- channel_gain: float32 [1536], P('tp'), may hold values from 0.1 to 1.9
- w_output: bfloat16 [1536, 2048], P('tp'), may hold values from -0.15625 to 0.15625
- expert_in: bfloat16 [1024, 2048], P('ep'), may hold values from -6 to 6
- expert_gain: float32 [2048], replicated, may hold values from 0 to 8
- route_experts: int32 [1024, 4], P('ep'), may hold values from 0 to 7, all different within a row; in each aligned block of 128 rows (0 to 127, 128 to 255, ...) at most 128 rows name the same one
- route_scores: float32 [1024, 4], P('ep'), may hold values from -6 to 6
- expert_gate: bfloat16 [8, 2048, 2048], P('ep', None, 'tp'), may hold values from -0.125 to 0.125
- expert_up: bfloat16 [8, 2048, 2048], P('ep', None, 'tp'), may hold values from -0.125 to 0.125
- expert_down: bfloat16 [8, 2048, 2048], P('ep', 'tp'), may hold values from -0.125 to 0.125
Outputs:
- mixer_out: bfloat16 [1024, 2048], P('ep')
- expert_out: bfloat16 [1024, 2048], P('ep')
Inputs may be any that keep to these rules, and one draw needn't show every extreme that they name: `route_experts`: each row names 4 different experts. In each aligned block of 128 rows (the rows of one index of ep) no expert is named more than 128 times, a bound that some block reaches.
All inputs are finite; a program needn't handle non-finite values.
Results may differ from a plain program's by a relative error of at most 0.02.
Values may be sent and summed in bfloat16 or wider, within the bound.
A program may use at most 64 MiB of HBM per device.

v0:
```python
import jax
import jax.numpy as jnp
from jax import lax
from jax.sharding import PartitionSpec as P

CONV_CH = 1536
CONV_W = 31
TOP_K = 4
epsilon = 1e-05
clamp_limit = 7.0
swish_slope = 1.702


def shifted(block, axis, distance):
    devices = range(lax.axis_size(axis))
    route = [(i - distance, i) for i in devices if i - distance in devices]
    return lax.ppermute(block, axis, route)


def row_norm(inputs, gains):
    widened = inputs.astype(jnp.float32)
    row_mean = jnp.mean(widened, axis=-1, keepdims=True)
    row_var = jnp.mean(jnp.square(widened - row_mean), axis=-1, keepdims=True)
    return (widened - row_mean) * lax.rsqrt(row_var + epsilon) * gains


def local(
    mixer_in,
    mixer_gain,
    w_value,
    w_gate,
    w_taps,
    channel_gain,
    w_output,
    expert_in,
    expert_gain,
    route_experts,
    route_scores,
    expert_gate,
    expert_up,
    expert_down,
):
    normed = row_norm(mixer_in, mixer_gain).astype(jnp.bfloat16)
    values = jnp.dot(normed, w_value, preferred_element_type=jnp.float32)
    gate_pre = jnp.dot(normed, w_gate, preferred_element_type=jnp.float32)
    gated_values = (values * jax.nn.sigmoid(gate_pre)).astype(jnp.bfloat16)
    mixer_rows = gated_values.shape[0]
    reach_rows = CONV_W - 1
    earlier = shifted(gated_values[mixer_rows - reach_rows :], "ep", 1)
    extended = jnp.concatenate([earlier, gated_values], axis=0)
    conv_out = jnp.zeros(gated_values.shape, jnp.float32)
    for offset in range(CONV_W):
        conv_out = (
            conv_out + extended[offset : offset + mixer_rows].astype(jnp.float32) * w_taps[offset]
        )
    channel_sums = lax.psum(
        (
            jnp.sum(conv_out, axis=1, keepdims=True),
            jnp.sum(conv_out * conv_out, axis=1, keepdims=True),
        ),
        "tp",
    )
    row_mean = channel_sums[0] / CONV_CH
    row_var = channel_sums[1] / CONV_CH - row_mean * row_mean
    activated = jax.nn.silu(
        (conv_out - row_mean) * lax.rsqrt(row_var + epsilon) * channel_gain
    ).astype(jnp.bfloat16)
    mixer_out = lax.psum(
        jnp.dot(activated, w_output, preferred_element_type=jnp.float32).astype(jnp.bfloat16), "tp"
    )
    rows_b = expert_in.shape[0]
    width = expert_in.shape[1]
    experts = lax.axis_size("ep")
    capacity = 2 * rows_b * TOP_K // experts
    slot_share = capacity // lax.axis_size("tp")
    column = lax.axis_index("tp")
    normed_b = row_norm(expert_in, expert_gain).astype(jnp.bfloat16)
    raised = jnp.exp(route_scores)
    route_weights = raised / jnp.sum(raised, axis=1, keepdims=True)
    flat_ids = route_experts.reshape(-1)
    onehot = (flat_ids[:, None] == jnp.arange(experts, dtype=jnp.int32)[None, :]).astype(jnp.int32)
    slot_index = jnp.sum((jnp.cumsum(onehot, axis=0) - onehot) * onehot, axis=1)
    owner_row = jnp.arange(rows_b * TOP_K, dtype=jnp.int32) // TOP_K
    slot_table = (
        jnp.full((capacity * experts,), rows_b, jnp.int32)
        .at[slot_index * experts + flat_ids]
        .set(owner_row)
    )
    padded = jnp.concatenate([normed_b, jnp.zeros((1, width), jnp.bfloat16)], axis=0)
    gate_w = expert_gate[0]
    up_w = expert_up[0]
    down_w = expert_down[0]
    own_table = lax.dynamic_slice_in_dim(
        slot_table, column * slot_share * experts, slot_share * experts
    )
    sending = jnp.take(padded, own_table, axis=0).reshape(slot_share, experts, width)
    arrived = lax.all_to_all(sending, "ep", split_axis=1, concat_axis=1, tiled=True)
    block_rows = lax.all_gather(arrived, "tp", axis=0, tiled=True)
    flat_rows = block_rows.reshape(block_rows.shape[0] * block_rows.shape[1], block_rows.shape[2])
    gate_e = jnp.minimum(
        jnp.dot(flat_rows, gate_w, preferred_element_type=jnp.float32), clamp_limit
    )
    up_e = jnp.clip(
        jnp.dot(flat_rows, up_w, preferred_element_type=jnp.float32), -clamp_limit, clamp_limit
    )
    hidden = (
        ((up_e + 1.0) * gate_e * jax.nn.sigmoid(swish_slope * gate_e))
        .astype(jnp.bfloat16)
        .reshape(block_rows.shape[0], block_rows.shape[1], gate_w.shape[1])
        .reshape(capacity * experts, gate_w.shape[1])
    )
    summed = lax.psum_scatter(
        jnp.dot(hidden, down_w, preferred_element_type=jnp.float32).astype(jnp.bfloat16),
        "tp",
        scatter_dimension=0,
        tiled=True,
    )
    returned = lax.all_to_all(
        summed.reshape(slot_share, experts, width), "ep", split_axis=1, concat_axis=1, tiled=True
    )
    every_slot = lax.all_gather(returned, "tp", axis=0, tiled=True).reshape(
        capacity * experts, width
    )
    picked = jnp.take(every_slot, slot_index * experts + flat_ids, axis=0)
    picked = picked.reshape(rows_b, TOP_K, width).astype(jnp.float32)
    expert_out = jnp.sum(picked * route_weights[:, :, None], axis=1).astype(jnp.bfloat16)
    return (mixer_out, expert_out)


def solution(mesh):
    in_specs = (
        P("ep", None),
        P(),
        P(None, "tp"),
        P(None, "tp"),
        P(None, "tp"),
        P("tp"),
        P("tp", None),
        P("ep", None),
        P(),
        P("ep", None),
        P("ep", None),
        P("ep", None, "tp"),
        P("ep", None, "tp"),
        P("ep", "tp", None),
    )
    out_specs = (P("ep", None), P("ep", None))
    return jax.shard_map(local, mesh=mesh, in_specs=in_specs, out_specs=out_specs, check_vma=False)
```

profile of v0, /device:TPU:0, one launch (start us, length us, event | category | flops | bytes accessed | tf_op | source)
XLA Modules:
  0.0 263.1 jit_solution(18099323295168561547)
XLA Ops:
  7.2 0.0 copy-start
  7.2 0.0 all-gather.3.cloned.1.call-start
  7.2 0.9 copy.33
  8.2 0.1 eq.29
  8.3 0.1 eq.25
  8.4 0.1 reshape.119
  8.5 1.1 reduce-window.6
  9.7 0.2 slice_reduce_fusion
  9.9 0.1 fusion.68
  10.0 2.4 scatter_custom_fusion
  12.5 0.1 compare_and_fusion
  12.6 1.2 convert_reduce_fusion
  13.8 1.3 fusion.24
  15.1 0.1 broadcast_in_dim.49
  15.2 0.1 copy.38
  15.3 1.4 fusion.26
  16.8 2.3 gather_fusion
  19.1 2.4 copy_select_fusion
  21.6 32.8 %all_to_all.10 = bf16[32,8,2048]{2,0,1:T(8,128)(2,1)S(1)} all-to-all(bf16[32,8,2048]{2,0,1:T(8,128)(2,1)S(1)} %copy_select_fusion), channel_id=1, replica_groups=mesh['ep'=8,'tp'=4] {'ep'}, dimensions={1} | all-to-all | bytes 2097152 | tf_op jit(solution)/shard_map/all_to_all | solution.py:97
  54.4 1.6 copy.40
  56.0 0.0 all-gather.3.cloned.1.call-update
  56.0 0.0 reduce-scatter.2.cloned.1.call-start
  56.0 33.6 %all-gather.3.cloned.1.call-done = bf16[128,8,2048]{2,1,0:T(8,128)(2,1)} async-done(((bf16[32,8,2048]{2,1,0:T(8,128)(2,1)}), bf16[128,8,2048]{2,1,0:T(8,128)(2,1)}) %all-gather.3.cloned.1.call-update) | async-done | bytes 4194320 | tf_op jit(solution)/shard_map/all_gather | solution.py:98
  89.7 6.6 %fusion.2 = f32[1024,512]{1,0:T(8,128)} fusion(bf16[128,8,2048]{2,1,0:T(8,128)(2,1)} %all-gather.3.cloned.1.call-done, bf16[1,2048,512]{2,1,0:T(8,128)(2,1)} %param.26), kind=kOutput, calls=%fused_computation.5 | convolution fusion | flops 2147483648 | bytes 8388608 | tf_op jit(solution)/shard_map/dot_general | solution.py:104
  96.2 0.0 copy-done
  96.2 10.3 %convolution_convert_fusion = bf16[1024,2048]{1,0:T(8,128)(2,1)} fusion(bf16[1,512,2048]{2,1,0:T(8,128)(2,1)S(1)} %copy-done, f32[1024,512]{1,0:T(8,128)} %fusion.2, bf16[1,2048,512]{2,1,0:T(8,128)(2,1)} %param.25, bf16[128,8,2048]{2,1,0:T(8,128)(2,1)} %all-gather.3.cloned.1.call-done), kind=kOutput, calls=%fused_computation.8 | convolution fusion | flops 4302307328 | bytes 14680064 | tf_op jit(solution)/shard_map/dot_general | solution.py:113
  106.5 0.0 reduce-scatter.2.cloned.1.call-update
  106.6 0.0 all-gather.5.cloned.1.call-start
  106.6 44.7 %reduce-scatter.2.cloned.1.call-done = bf16[256,2048]{1,0:T(8,128)(2,1)} async-done(((bf16[1024,2048]{1,0:T(8,128)(2,1)}), bf16[256,2048]{1,0:T(8,128)(2,1)}) %reduce-scatter.2.cloned.1.call-update) | async-done | bytes 1048592 | tf_op jit(solution)/shard_map/reduce_scatter | solution.py:112
  151.3 1.8 copy.41
  153.1 30.9 %all_to_all.11 = bf16[32,8,2048]{2,0,1:T(8,128)(2,1)S(1)} all-to-all(bf16[32,8,2048]{2,0,1:T(8,128)(2,1)S(1)} %copy.41), channel_id=1, replica_groups=mesh['ep'=8,'tp'=4] {'ep'}, dimensions={1} | all-to-all | bytes 2097152 | tf_op jit(solution)/shard_map/all_to_all | solution.py:118
  184.0 1.6 copy.42
  185.6 0.0 all-gather.5.cloned.1.call-update
  185.6 0.2 all-reduce.4.cloned.1.call-start
  185.9 0.0 copy-start.5
  185.9 0.2 convert_reduce_fusion.1
  186.0 0.3 fusion.27
  186.3 1.9 fusion.81
  188.2 0.0 copy-done.5
  188.3 0.0 copy-start.4
  188.3 0.0 copy-start.2
  188.3 0.0 copy-start.3
  188.3 0.0 copy-start.7
  188.3 0.5 fusion.23
  188.9 3.4 %collective-permute-start = (bf16[30,384]{1,0:T(8,128)(2,1)S(1)}, bf16[30,384]{1,0:T(8,128)(2,1)S(1)}, u32[]{:S(2)}, u32[]{:S(2)}) collective-permute-start(bf16[30,384]{1,0:T(8,128)(2,1)S(1)} %slice.260), channel_id=1, source_target_pairs={{0,4},{4,8},{8,12},{12,16},{16,20},{20,24},{24,28},{1,5},{5,9},{9,... | collective-permute-start | bytes 69128 | tf_op jit(solution)/shard_map/ppermute | solution.py:17
  192.2 0.1 mul.528
  192.4 0.1 copy.35
  192.5 0.1 slice_reduce_fusion.30
  192.5 0.1 slice_reduce_fusion.31
  192.6 0.0 copy-done.3
  192.7 0.1 copy.36
  192.8 0.1 copy.43
  192.9 0.8 collective-permute-done
  193.7 0.9 fusion.83
  194.7 6.5 %all-reduce.1 = (f32[128,1]{0,1:T(1,128)S(1)}, f32[128,1]{0,1:T(1,128)S(1)}) all-reduce(f32[128,1]{0,1:T(1,128)S(1)} %bitcast.51, f32[128,1]{0,1:T(1,128)S(1)} %bitcast.50), channel_id=1, replica_groups=mesh['ep'=8,'tp'=4] {'tp'}, use_global_device_ids=true, to_apply=%region_5.0 | all-reduce | flops 256 | bytes 2048 | tf_op jit(solution)/shard_map/psum | solution.py:56
  201.1 0.0 copy-done.7
  201.1 2.7 %convolution_convert_fusion.1 = bf16[128,2048]{1,0:T(8,128)(2,1)} fusion(bf16[384,2048]{1,0:T(8,128)(2,1)} %param.20, f32[128,384]{1,0:T(8,128)S(1)} %get-tuple-element.39, f32[384]{0:T(512)S(1)} %copy-done.7, f32[128]{0:T(128)S(1)} %get-tuple-element.41, f32[128]{0:T(128)S(1)} %get-tuple-element.40), kind=kOutput, calls=%fused_computation.9 | convolution fusion | flops 201981952 | bytes 2296320 | tf_op jit(solution)/shard_map/dot_general | solution.py:69
  203.9 0.0 all-reduce.4.cloned.1.call-update
  203.9 14.5 %all-gather.5.cloned.1.call-done = bf16[128,8,2048]{2,1,0:T(8,128)(2,1)} async-done(((bf16[32,8,2048]{2,1,0:T(8,128)(2,1)}), bf16[128,8,2048]{2,1,0:T(8,128)(2,1)}) %all-gather.5.cloned.1.call-update) | async-done | bytes 4194320 | tf_op jit(solution)/shard_map/all_gather | solution.py:121
  218.4 8.0 %gather_fusion.1 = bf16[512,2048]{1,0:T(8,128)(2,1)} fusion(bf16[1024,2048]{1,0:T(8,128)(2,1)} %bitcast.44, s32[1024]{0:T(1024)S(1)} %pad_clamp_fusion), kind=kCustom, calls=%fused_computation.1 | custom fusion | bytes 4196352 | tf_op jit(solution)/shard_map/jit(_take)/gather | solution.py:124
  226.4 4.1 %gather.15 = bf16[128,4,2048]{2,1,0:T(4,128)(2,1)} reshape(bf16[512,2048]{1,0:T(8,128)(2,1)} %gather_fusion.1) | data formatting | bytes 4194304 | tf_op jit(solution)/shard_map/jit(_take)/gather | solution.py:124
  230.6 6.4 %multiply_reduce_fusion = bf16[128,2048]{1,0:T(8,128)(2,1)} fusion(f32[128,4]{1,0:T(8,128)S(1)} %copy.43, bf16[128,4,2048]{2,1,0:T(4,128)(2,1)} %gather.15, pred[128,4]{1,0:T(8,128)(4,1)S(1)} %copy.36), kind=kLoop, calls=%fused_computation.7 | loop fusion | flops 3932160 | bytes 2624000 | tf_op jit(solution)/shard_map/reduce_sum | solution.py:126
  237.0 17.7 %all-reduce.4.cloned.1.call-done = bf16[128,2048]{1,0:T(8,128)(2,1)} async-done(((bf16[128,2048]{1,0:T(8,128)(2,1)}), bf16[128,2048]{1,0:T(8,128)(2,1)}) %all-reduce.4.cloned.1.call-update) | async-done | bytes 524304 | tf_op jit(solution)/shard_map/psum | solution.py:68
  254.7 1.9 copy.46
  (24 shorter events, 0.2 us)
Async XLA Ops:
  7.2 89.1 %copy-start = (bf16[1,512,2048]{2,1,0:T(8,128)(2,1)S(1)}, bf16[1,512,2048]{2,1,0:T(8,128)(2,1)}, u32[]{:S(2)}) copy-start(bf16[1,512,2048]{2,1,0:T(8,128)(2,1)} %param.27) | copy-start | bytes 6291460
  7.2 82.5 %all-gather.3.cloned.1.call-start = ((), (), s32[]{:S(2)}) async-start(), calls=%async_computation.4 | async-start | bytes 5242880 | tf_op jit(solution)/shard_map/all_gather | solution.py:98
  56.0 95.3 %reduce-scatter.2.cloned.1.call-start = ((), (), s32[]{:S(2)}) async-start(), calls=%async_computation.5 | async-start | bytes 5242880 | tf_op jit(solution)/shard_map/reduce_scatter | solution.py:112
  106.6 111.9 %all-gather.5.cloned.1.call-start = ((), (), s32[]{:S(2)}) async-start(), calls=%async_computation.6 | async-start | bytes 5242880 | tf_op jit(solution)/shard_map/all_gather | solution.py:121
  184.0 1.8 copy-start.1
  184.0 2.3 copy-start.6
  185.6 69.1 %all-reduce.4.cloned.1.call-start = ((), (), s32[]{:S(2)}) async-start(), calls=%async_computation.3 | async-start | bytes 1048576 | tf_op jit(solution)/shard_map/psum | solution.py:68
  185.9 2.4 copy-start.5
  188.3 4.2 %copy-start.4 = (f32[128,4]{0,1:T(4,128)S(1)}, f32[128,4]{0,1:T(4,128)}, u32[]{:S(2)}) copy-start(f32[128,4]{0,1:T(4,128)} %param.24) | copy-start | bytes 6148
  188.3 4.2 %copy-start.2 = (f32[31,384]{1,0:T(8,128)S(1)}, f32[31,384]{1,0:T(8,128)}, u32[]{:S(2)}) copy-start(f32[31,384]{1,0:T(8,128)} %param.18) | copy-start | bytes 142852
  188.3 4.4 %copy-start.3 = (s32[128,4]{0,1:T(4,128)S(1)}, s32[128,4]{0,1:T(4,128)}, u32[]{:S(2)}) copy-start(s32[128,4]{0,1:T(4,128)} %param.23) | copy-start | bytes 6148
  188.3 12.9 %copy-start.7 = (f32[384]{0:T(512)S(1)}, f32[384]{0:T(512)}, u32[]{:S(2)}) copy-start(f32[384]{0:T(512)} %param.19) | copy-start | bytes 4612
  188.9 4.9 %collective-permute-start = (bf16[30,384]{1,0:T(8,128)(2,1)S(1)}, bf16[30,384]{1,0:T(8,128)(2,1)S(1)}, u32[]{:S(2)}, u32[]{:S(2)}) collective-permute-start(bf16[30,384]{1,0:T(8,128)(2,1)S(1)} %slice.260), channel_id=1, source_target_pairs={{0,4},{4,8},{8,12},{12,16},{16,20},{20,24},{24,28},{1,5},{5,9},{9,... | collective-permute-start | bytes 69128 | tf_op jit(solution)/shard_map/ppermute | solution.py:17
Sparse Core Ops, SparseCore 0:
  56.1 33.4 all-gather.2
  106.7 44.5 reduce-scatter.1
  185.7 32.6 all-gather.4
  221.2 33.4 all-reduce.3
where the time goes:
time: 264 us; the launch traced here: 263 us
  waiting for transfers between devices  111 us (42%)
  blocking collectives  70.2 us (27%)
  local copies, waits for them, and re-layouts  26 us (10%)
  matrix products  22.1 us (8%)
  other arithmetic  15.7 us (6%)
  between operations  14 us (5%)
  starting transfers between devices  3.71 us (1%)
    reduce_scatter x1, waiting for transfers between devices, local(): lax.psum_scatter(jnp.dot(hidden, down_w, preferred_element_type=jnp.float...  44.7 us
    all_gather x1, waiting for transfers between devices, local(): block_rows = lax.all_gather(arrived, 'tp', axis=0, tiled=True)  33.6 us
    all_to_all x1, blocking collectives, local(): lax.all_to_all(sending, 'ep', split_axis=1, concat_axis=1, tiled=True)  32.8 us
    all_to_all x1, blocking collectives, local(): lax.all_to_all(summed.reshape(slot_share, experts, width), 'ep', split_ax...  30.9 us
    psum x1, waiting for transfers between devices, local(): lax.psum(jnp.dot(activated, w_output, preferred_element_type=jnp.float32)...  17.7 us
    all_gather x1, waiting for transfers between devices, local(): lax.all_gather(returned, 'tp', axis=0, tiled=True)  14.5 us
    gather x2, local copies, waits for them, and re-layouts, local(): picked = jnp.take(every_slot, slot_index * experts + flat_ids, axis=0)  12.1 us
    dot_general x1, matrix products, local(): jnp.dot(hidden, down_w, preferred_element_type=jnp.float32)  10.3 us
  transfers between devices with their start and end apart: 5, of which 5 were waited for; matrix products, arithmetic and copies ran while one was open for 10% of the time, Pallas kernels for 0%

commit v1 on v0

--- a/solution.py
+++ b/solution.py
@@ -65,9 +65,10 @@
     activated = jax.nn.silu(
         (conv_out - row_mean) * lax.rsqrt(row_var + epsilon) * channel_gain
     ).astype(jnp.bfloat16)
-    mixer_out = lax.psum(
-        jnp.dot(activated, w_output, preferred_element_type=jnp.float32).astype(jnp.bfloat16), "tp"
+    local_array = jnp.dot(activated, w_output, preferred_element_type=jnp.float32).astype(
+        jnp.bfloat16
     )
+    mixer_out = lax.all_gather(local_array, axis_name="tp").sum(axis=0)
     rows_b = expert_in.shape[0]
     width = expert_in.shape[1]
     experts = lax.axis_size("ep")

time: 264 us -> 244 us (0.924)
  waiting for transfers between devices: 111 us -> 90.2 us
  other arithmetic: 15.7 us -> 18.6 us
    reduce_scatter x1, waiting for transfers between devices: 44.7 us -> 26.2 us  [local(): lax.psum_scatter(jnp.dot(hidden, down_w, preferred_element_type=jnp.float...]
    psum x1 -> x0, waiting for transfers between devices: 17.7 us -> none  [local(): lax.psum(jnp.dot(activated, w_output, preferred_element_type=jnp.float32)...]
    all_gather x1, waiting for transfers between devices: 14.5 us -> 29.2 us  [local(): lax.all_gather(returned, 'tp', axis=0, tiled=True)]
    reduce_sum x0 -> x1, other arithmetic: none -> 2.92 us  [local(): mixer_out = lax.all_gather(local_array, axis_name='tp').sum(axis=0)]
  transfers between devices with their start and end apart: 5 -> 5, of which waited for: 5 -> 4; matrix products, arithmetic and copies ran while one was open for 10% -> 6% of each run, Pallas kernels for 0% -> 0%
where the time goes in v1:
time: 244 us; the launch traced here: 243 us
  waiting for transfers between devices  90.2 us (37%)
  blocking collectives  69.7 us (29%)
  local copies, waits for them, and re-layouts  25.1 us (10%)
  matrix products  22 us (9%)
  other arithmetic  18.6 us (8%)
  between operations  14 us (6%)
  starting transfers between devices  3.71 us (2%)
    all_gather x1, waiting for transfers between devices, local(): block_rows = lax.all_gather(arrived, 'tp', axis=0, tiled=True)  33.6 us
    all_to_all x1, blocking collectives, local(): lax.all_to_all(sending, 'ep', split_axis=1, concat_axis=1, tiled=True)  32.8 us
    all_to_all x1, blocking collectives, local(): lax.all_to_all(summed.reshape(slot_share, experts, width), 'ep', split_ax...  30.9 us
    all_gather x1, waiting for transfers between devices, local(): lax.all_gather(returned, 'tp', axis=0, tiled=True)  29.2 us
    reduce_scatter x1, waiting for transfers between devices, local(): lax.psum_scatter(jnp.dot(hidden, down_w, preferred_element_type=jnp.float...  26.2 us
    gather x2, local copies, waits for them, and re-layouts, local(): picked = jnp.take(every_slot, slot_index * experts + flat_ids, axis=0)  12.1 us
    dot_general x1, matrix products, local(): jnp.dot(hidden, down_w, preferred_element_type=jnp.float32)  10.3 us
    dot_general x1, matrix products, local(): jnp.dot(flat_rows, up_w, preferred_element_type=jnp.float32)  6.59 us
  transfers between devices with their start and end apart: 5, of which 4 were waited for; matrix products, arithmetic and copies ran while one was open for 6% of the time, Pallas kernels for 0%

profile of v1, /device:TPU:0, one launch (start us, length us, event | category | flops | bytes accessed | tf_op | source)
XLA Modules:
  0.0 243.4 jit_solution(6394160969569035820)
XLA Ops:
  7.2 0.0 copy-start
  7.2 0.0 all-gather.5.cloned.1.call-start
  7.2 0.9 copy.33
  8.2 0.1 eq.29
  8.3 0.1 eq.25
  8.4 0.1 reshape.119
  8.5 1.1 reduce-window.6
  9.7 0.2 slice_reduce_fusion
  9.9 0.1 fusion.68
  10.0 2.4 %scatter_custom_fusion = s32[1024]{0:T(1024)S(1)} fusion(s32[512]{0:T(512)S(1)} %bitcast.50, s32[512]{0:T(512)S(1)} %add_select_fusion, s32[]{:T(128)} %constant.84.clone.1), kind=kCustom, calls=%fused_computation.150 | custom fusion | bytes 4100 | tf_op jit(solution)/shard_map/scatter | solution.py:88
  12.5 0.1 compare_and_fusion
  12.6 1.2 convert_reduce_fusion
  13.8 1.3 fusion.24
  15.1 0.1 broadcast_in_dim.49
  15.2 0.1 copy.38
  15.3 1.4 fusion.26
  16.8 2.3 gather_fusion
  19.1 2.4 %copy_select_fusion = bf16[32,8,2048]{2,0,1:T(8,128)(2,1)S(1)} fusion(bf16[32,8,2048]{2,1,0:T(8,128)(2,1)} %bitcast.46, pred[32,8]{0,1:T(8,128)(4,1)S(1)} %copy.38), kind=kLoop, calls=%fused_computation.63 | loop fusion | flops 524288 | bytes 2097408 | tf_op jit(solution)/shard_map/jit(_take)/select_n | solution.py:97
  21.6 32.8 %all_to_all.10 = bf16[32,8,2048]{2,0,1:T(8,128)(2,1)S(1)} all-to-all(bf16[32,8,2048]{2,0,1:T(8,128)(2,1)S(1)} %copy_select_fusion), channel_id=1, replica_groups=mesh['ep'=8,'tp'=4] {'ep'}, dimensions={1} | all-to-all | bytes 2097152 | tf_op jit(solution)/shard_map/all_to_all | solution.py:98
  54.4 1.6 copy.40
  56.0 0.0 all-gather.5.cloned.1.call-update
  56.0 0.0 reduce-scatter.2.cloned.1.call-start
  56.1 33.6 %all-gather.5.cloned.1.call-done = bf16[128,8,2048]{2,1,0:T(8,128)(2,1)} async-done(((bf16[32,8,2048]{2,1,0:T(8,128)(2,1)}), bf16[128,8,2048]{2,1,0:T(8,128)(2,1)}) %all-gather.5.cloned.1.call-update) | async-done | bytes 4194320 | tf_op jit(solution)/shard_map/all_gather | solution.py:99
  89.7 6.6 %fusion.2 = f32[1024,512]{1,0:T(8,128)} fusion(bf16[128,8,2048]{2,1,0:T(8,128)(2,1)} %all-gather.5.cloned.1.call-done, bf16[1,2048,512]{2,1,0:T(8,128)(2,1)} %param.26), kind=kOutput, calls=%fused_computation.5 | convolution fusion | flops 2147483648 | bytes 8388608 | tf_op jit(solution)/shard_map/dot_general | solution.py:105
  96.3 0.0 copy-done
  96.3 10.3 %convolution_convert_fusion = bf16[1024,2048]{1,0:T(8,128)(2,1)} fusion(bf16[1,512,2048]{2,1,0:T(8,128)(2,1)S(1)} %copy-done, f32[1024,512]{1,0:T(8,128)} %fusion.2, bf16[1,2048,512]{2,1,0:T(8,128)(2,1)} %param.25, bf16[128,8,2048]{2,1,0:T(8,128)(2,1)} %all-gather.5.cloned.1.call-done), kind=kOutput, calls=%fused_computation.8 | convolution fusion | flops 4302307328 | bytes 14680064 | tf_op jit(solution)/shard_map/dot_general | solution.py:114
  106.5 0.0 reduce-scatter.2.cloned.1.call-update
  106.5 0.0 all-gather.9.cloned.1.call-start
  106.6 1.0 copy-done.1
  107.6 0.2 convert_reduce_fusion.1
  107.7 0.3 fusion.27
  108.0 0.0 copy-done.6
  108.0 1.9 fusion.81
  109.9 0.0 copy-done.5
  109.9 0.0 copy-start.2
  110.0 0.0 copy-start.7
  110.0 0.5 fusion.23
  110.5 3.5 %collective-permute-start = (bf16[30,384]{1,0:T(8,128)(2,1)S(1)}, bf16[30,384]{1,0:T(8,128)(2,1)S(1)}, u32[]{:S(2)}, u32[]{:S(2)}) collective-permute-start(bf16[30,384]{1,0:T(8,128)(2,1)S(1)} %slice.260), channel_id=1, source_target_pairs={{0,4},{4,8},{8,12},{12,16},{16,20},{20,24},{24,28},{1,5},{5,9},{9,... | collective-permute-start | bytes 69128 | tf_op jit(solution)/shard_map/ppermute | solution.py:17
  114.1 0.0 copy-done.2
  114.1 0.1 slice_reduce_fusion.31
  114.2 0.1 slice_reduce_fusion.30
  114.3 1.1 collective-permute-done
  115.4 0.9 fusion.83
  116.3 6.0 %all-reduce.1 = (f32[128,1]{0,1:T(1,128)S(1)}, f32[128,1]{0,1:T(1,128)S(1)}) all-reduce(f32[128,1]{0,1:T(1,128)S(1)} %bitcast.53, f32[128,1]{0,1:T(1,128)S(1)} %bitcast.52), channel_id=1, replica_groups=mesh['ep'=8,'tp'=4] {'tp'}, use_global_device_ids=true, to_apply=%region_5.0 | all-reduce | flops 256 | bytes 2048 | tf_op jit(solution)/shard_map/psum | solution.py:56
  122.3 0.0 copy-done.7
  122.3 2.7 %convolution_convert_fusion.1 = bf16[128,2048]{1,0:T(8,128)(2,1)} fusion(bf16[384,2048]{1,0:T(8,128)(2,1)} %param.20, f32[128,384]{1,0:T(8,128)S(1)} %get-tuple-element.39, f32[384]{0:T(512)S(1)} %copy-done.7, f32[128]{0:T(128)S(1)} %get-tuple-element.41, f32[128]{0:T(128)S(1)} %get-tuple-element.40), kind=kOutput, calls=%fused_computation.9 | convolution fusion | flops 201981952 | bytes 2296320 | tf_op jit(solution)/shard_map/dot_general | solution.py:68
  125.0 0.0 all-gather.9.cloned.1.call-update
  125.1 0.0 all-gather.7.cloned.1.call-start
  125.1 26.2 %reduce-scatter.2.cloned.1.call-done = bf16[256,2048]{1,0:T(8,128)(2,1)} async-done(((bf16[1024,2048]{1,0:T(8,128)(2,1)}), bf16[256,2048]{1,0:T(8,128)(2,1)}) %reduce-scatter.2.cloned.1.call-update) | async-done | bytes 1048592 | tf_op jit(solution)/shard_map/reduce_scatter | solution.py:113
  151.3 1.8 copy.41
  153.1 30.9 %all_to_all.11 = bf16[32,8,2048]{2,0,1:T(8,128)(2,1)S(1)} all-to-all(bf16[32,8,2048]{2,0,1:T(8,128)(2,1)S(1)} %copy.41), channel_id=1, replica_groups=mesh['ep'=8,'tp'=4] {'ep'}, dimensions={1} | all-to-all | bytes 2097152 | tf_op jit(solution)/shard_map/all_to_all | solution.py:119
  184.0 1.6 copy.42
  185.6 0.0 all-gather.7.cloned.1.call-update
  185.6 0.1 mul.528
  185.7 0.1 copy.35
  185.8 0.0 copy-done.3
  185.8 0.1 copy.36
  186.0 0.1 copy.43
  186.1 0.0 all-gather.9.cloned.1.call-done
  186.1 2.9 %reduce_sum.97 = bf16[128,2048]{1,0:T(8,128)(2,1)} reduce(bf16[4,128,2048]{2,1,0:T(8,128)(2,1)} %bitcast.47, bf16[]{:T(256)} %constant.78.clone.1), dimensions={0}, to_apply=%region_6.7 | reduce | flops 786432 | bytes 2621442 | tf_op jit(solution)/shard_map/reduce_sum | solution.py:71
  189.1 29.2 %all-gather.7.cloned.1.call-done = bf16[128,8,2048]{2,1,0:T(8,128)(2,1)} async-done(((bf16[32,8,2048]{2,1,0:T(8,128)(2,1)}), bf16[128,8,2048]{2,1,0:T(8,128)(2,1)}) %all-gather.7.cloned.1.call-update) | async-done | bytes 4194320 | tf_op jit(solution)/shard_map/all_gather | solution.py:122
  218.3 8.0 %gather_fusion.1 = bf16[512,2048]{1,0:T(8,128)(2,1)} fusion(bf16[1024,2048]{1,0:T(8,128)(2,1)} %bitcast.45, s32[1024]{0:T(1024)S(1)} %pad_clamp_fusion), kind=kCustom, calls=%fused_computation.1 | custom fusion | bytes 4196352 | tf_op jit(solution)/shard_map/jit(_take)/gather | solution.py:125
  226.3 4.1 %gather.15 = bf16[128,4,2048]{2,1,0:T(4,128)(2,1)} reshape(bf16[512,2048]{1,0:T(8,128)(2,1)} %gather_fusion.1) | data formatting | bytes 4194304 | tf_op jit(solution)/shard_map/jit(_take)/gather | solution.py:125
  230.4 6.4 %multiply_reduce_fusion = bf16[128,2048]{1,0:T(8,128)(2,1)} fusion(f32[128,4]{1,0:T(8,128)S(1)} %copy.43, bf16[128,4,2048]{2,1,0:T(4,128)(2,1)} %gather.15, pred[128,4]{1,0:T(8,128)(4,1)S(1)} %copy.36), kind=kLoop, calls=%fused_computation.7 | loop fusion | flops 3932160 | bytes 2624000 | tf_op jit(solution)/shard_map/reduce_sum | solution.py:127
  (24 shorter events, 0.2 us)
Async XLA Ops:
  7.2 89.1 %copy-start = (bf16[1,512,2048]{2,1,0:T(8,128)(2,1)S(1)}, bf16[1,512,2048]{2,1,0:T(8,128)(2,1)}, u32[]{:S(2)}) copy-start(bf16[1,512,2048]{2,1,0:T(8,128)(2,1)} %param.27) | copy-start | bytes 6291460
  7.2 82.5 %all-gather.5.cloned.1.call-start = ((), (), s32[]{:S(2)}) async-start(), calls=%async_computation.3 | async-start | bytes 5242880 | tf_op jit(solution)/shard_map/all_gather | solution.py:99
  56.0 95.2 %reduce-scatter.2.cloned.1.call-start = ((), (), s32[]{:S(2)}) async-start(), calls=%async_computation.4 | async-start | bytes 5242880 | tf_op jit(solution)/shard_map/reduce_scatter | solution.py:113
  106.5 1.0 copy-start.1
  106.5 1.5 copy-start.6
  106.5 79.6 %all-gather.9.cloned.1.call-start = ((), (), s32[]{:S(2)}) async-start(), calls=%async_computation.6 | async-start | bytes 2621440 | tf_op jit(solution)/shard_map/all_gather | solution.py:71
  107.6 2.4 copy-start.5
  109.9 4.1 %copy-start.2 = (f32[31,384]{1,0:T(8,128)S(1)}, f32[31,384]{1,0:T(8,128)}, u32[]{:S(2)}) copy-start(f32[31,384]{1,0:T(8,128)} %param.18) | copy-start | bytes 142852
  110.0 12.4 %copy-start.7 = (f32[384]{0:T(512)S(1)}, f32[384]{0:T(512)}, u32[]{:S(2)}) copy-start(f32[384]{0:T(512)} %param.19) | copy-start | bytes 4612
  110.5 4.9 %collective-permute-start = (bf16[30,384]{1,0:T(8,128)(2,1)S(1)}, bf16[30,384]{1,0:T(8,128)(2,1)S(1)}, u32[]{:S(2)}, u32[]{:S(2)}) collective-permute-start(bf16[30,384]{1,0:T(8,128)(2,1)S(1)} %slice.260), channel_id=1, source_target_pairs={{0,4},{4,8},{8,12},{12,16},{16,20},{20,24},{24,28},{1,5},{5,9},{9,... | collective-permute-start | bytes 69128 | tf_op jit(solution)/shard_map/ppermute | solution.py:17
  125.1 93.2 %all-gather.7.cloned.1.call-start = ((), (), s32[]{:S(2)}) async-start(), calls=%async_computation.5 | async-start | bytes 5242880 | tf_op jit(solution)/shard_map/all_gather | solution.py:122
  184.0 1.8 copy-start.3
  184.0 2.0 copy-start.4
Sparse Core Ops, SparseCore 0:
  56.1 33.4 all-gather.4
  106.7 44.5 reduce-scatter.1
  153.4 22.5 all-gather.8
  185.7 32.5 all-gather.6
